TPU v7x, 32 devices: a whole 2x2x4 slice. The times are simulated.
32 devices in a mesh: sp: 16 (over z, y, x), tp: 2 (over core).
Axes of the slice: x: 2, y: 2, z: 4, core: 2. Of those that a mesh axis runs over, the one named last changes fastest.
Arguments:
- hidden_in: bfloat16 [4096, 2048], P('sp'), may hold values from -16 to 16
- query_one: bfloat16 [2048, 512], P(None, 'tp'), may hold values from -0.13258252 to 0.13258252
- query_two: bfloat16 [2048, 512], P(None, 'tp'), may hold values from -0.13258252 to 0.13258252
- key_one: bfloat16 [2048, 512], P(None, 'tp'), may hold values from -0.13258252 to 0.13258252
- key_two: bfloat16 [2048, 512], P(None, 'tp'), may hold values from -0.13258252 to 0.13258252
- value_proj: bfloat16 [2048, 1024], P(None, 'tp'), may hold values from -0.125 to 0.125
- lambdas: float32 [8], P('tp'), may hold values from 0.3 to 0.8
- norm_gain: float32 [128], replicated, may hold values from 0.1 to 1.9
- out_proj: bfloat16 [1024, 2048], P('tp'), may hold values from -0.1875 to 0.1875
Outputs:
- attended: bfloat16 [4096, 2048], P('sp')
All inputs are finite; a program needn't handle non-finite values.
Results may differ from a plain program's by a relative error of at most 0.015.
Values may be sent and summed in bfloat16 or wider, within the bound.
A program may use at most 64 MiB of HBM per device.

v0:
```python
import math

import jax
import jax.numpy as jnp
from jax import lax
from jax.sharding import PartitionSpec as P

epsilon = 1e-06
masked_score = -1e30


def shards(
    hidden_in, query_one, query_two, key_one, key_two, value_proj, lambdas, norm_gain, out_proj
):
    heads_dev = lambdas.shape[0]
    head_qk = query_one.shape[1] // heads_dev
    head_v = value_proj.shape[1] // heads_dev
    width_q = heads_dev * head_qk
    score_scale = 1.75 * head_qk ** (-0.5)
    joined = jnp.concatenate((query_one, query_two, key_one, key_two, value_proj), axis=1)
    projected = jnp.dot(hidden_in, joined, preferred_element_type=jnp.float32).astype(jnp.bfloat16)
    tok_rows = projected.shape[0]
    key_values = projected[:, 2 * width_q :]
    my_index = lax.axis_index("sp")
    offset = my_index * tok_rows
    query_sets = (projected[:, : 2 * width_q],)
    position_sets = (offset + jnp.arange(tok_rows, dtype=jnp.int32),)
    groups = []
    for query_rows, positions in zip(query_sets, position_sets):
        group_rows = query_rows.shape[0]
        query_a = query_rows[:, :width_q].reshape(group_rows, heads_dev, head_qk)
        query_b = query_rows[:, width_q:].reshape(group_rows, heads_dev, head_qk)
        groups.append((query_a, query_b, positions, positions[group_rows - 1]))

    def one_map(queries, keys, value_rows, allowed, running_max, running_sum, accum):
        scores = (
            jnp.einsum("qhd,khd->hqk", queries, keys, preferred_element_type=jnp.float32)
            * score_scale
        )
        scores = jnp.where(allowed[None], scores, masked_score)
        new_max = jnp.maximum(running_max, jnp.max(scores, axis=-1))
        rescale = jnp.exp(running_max - new_max)
        weights = jnp.where(allowed[None], jnp.exp(scores - new_max[..., None]), 0.0)
        new_sum = running_sum * rescale + jnp.sum(weights, axis=-1)
        added = jnp.einsum(
            "hqk,khe->hqe",
            weights.astype(jnp.bfloat16),
            value_rows,
            preferred_element_type=jnp.float32,
        )
        return (new_max, new_sum, accum * rescale[..., None] + added)

    def absorb(group_state, group, kblock, kstart):
        query_a, query_b, positions, last_pos = group
        block_rows = kblock.shape[0]
        k_pos = kstart + jnp.arange(block_rows, dtype=jnp.int32)
        allowed = k_pos[None, :] <= positions[:, None]
        keys_a = kblock[:, :width_q].reshape(block_rows, heads_dev, head_qk)
        keys_b = kblock[:, width_q : 2 * width_q].reshape(block_rows, heads_dev, head_qk)
        value_rows = kblock[:, 2 * width_q :].reshape(block_rows, heads_dev, head_v)
        first_map = one_map(query_a, keys_a, value_rows, allowed, *group_state[:3])
        second_map = one_map(query_b, keys_b, value_rows, allowed, *group_state[3:])
        return first_map + second_map

    group = groups[0]
    group_rows = group[0].shape[0]
    start_max = jnp.full((heads_dev, group_rows), masked_score, jnp.float32)
    start_sum = jnp.zeros((heads_dev, group_rows), jnp.float32)
    start_acc = jnp.zeros((heads_dev, group_rows, head_v), jnp.float32)
    initial_list = [(start_max, start_sum, start_acc, start_max, start_sum, start_acc)]
    initial = tuple(initial_list)
    softmax_state = initial
    kv_piece = lax.all_gather(key_values, "sp", axis=0, tiled=True)
    piece_rows = kv_piece.shape[0]
    block_rows = math.gcd(piece_rows, 512)
    block_count = piece_rows // block_rows
    stacked = kv_piece.reshape(block_count, block_rows, kv_piece.shape[1])

    def absorb_step(carried, blocks_in):
        kblock, block_index = blocks_in
        kstart = block_index * block_rows
        renewed = []
        for group, group_state in zip(groups, carried):
            renewed.append(
                lax.cond(
                    kstart <= group[3],
                    lambda inner, group=group: absorb(inner, group, kblock, kstart),
                    lambda inner: inner,
                    group_state,
                )
            )
        return (tuple(renewed), None)

    softmax_state, _ = lax.scan(
        absorb_step, softmax_state, (stacked, jnp.arange(block_count, dtype=jnp.int32))
    )
    normed_sets = []
    for group_state in softmax_state:
        out_a = group_state[2] / group_state[1][..., None]
        out_b = group_state[5] / group_state[4][..., None]
        mixed_out = out_a - lambdas[:, None, None] * out_b
        scale_rows = lax.rsqrt(jnp.mean(mixed_out * mixed_out, axis=-1, keepdims=True) + epsilon)
        normed = (mixed_out * scale_rows * norm_gain).astype(jnp.bfloat16)
        group_rows = normed.shape[1]
        normed_sets.append(jnp.transpose(normed, (1, 0, 2)).reshape(group_rows, heads_dev * head_v))
    normed_all = normed_sets[0]
    partial_value = jnp.dot(normed_all, out_proj, preferred_element_type=jnp.float32)
    result = lax.psum(partial_value.astype(jnp.bfloat16), "tp")
    return result


def solution(mesh):
    placed = (
        P("sp", None),
        P(None, "tp"),
        P(None, "tp"),
        P(None, "tp"),
        P(None, "tp"),
        P(None, "tp"),
        P("tp"),
        P(),
        P("tp", None),
    )
    return jax.shard_map(
        shards, mesh=mesh, in_specs=placed, out_specs=P("sp", None), check_vma=False
    )
```

profile of v0, /device:TPU:0, one launch (start us, length us, event | category | flops | bytes accessed | tf_op | source)
XLA Modules:
  0.0 254.4 jit_solution(17439998530829736582)
XLA Ops:
  6.5 0.0 copy-start
  6.5 0.0 all-gather.2.cloned.1.call-start
  6.5 1.5 constant_dynamic-update-slice_fusion.4
  8.0 0.2 copy-done.2
  8.2 0.1 constant_dynamic-update-slice_fusion.3
  8.3 0.2 copy-done.3
  8.5 0.1 constant_dynamic-update-slice_fusion.2
  8.6 0.9 copy-done.4
  9.5 0.1 constant_dynamic-update-slice_fusion.1
  9.6 0.6 copy-done.1
  10.2 0.1 constant_dynamic-update-slice_fusion
  10.3 1.1 copy-done.7
  11.4 1.8 fusion.24
  13.3 0.8 slice.34
  14.1 0.0 all-gather.2.cloned.1.call-update
  14.1 0.0 all-reduce.2.cloned.1.call-start
  14.2 0.7 slice.27
  14.9 136.6 %all-gather.2.cloned.1.call-done = bf16[4096,1024]{0,1:T(8,128)(2,1)} async-done(((bf16[256,1024]{0,1:T(8,128)(2,1)}), bf16[4096,1024]{0,1:T(8,128)(2,1)}) %all-gather.2.cloned.1.call-update) | async-done | bytes 8388624 | tf_op jit(solution)/shard_map/all_gather | solution.py:73
  151.5 7.4 %copy.26 = bf16[128,8,8,512]{3,2,0,1:T(8,128)(2,1)} copy(bf16[128,8,8,512]{3,2,1,0:T(8,128)(2,1)} %bitcast.57) | data formatting | bytes 16777216 | tf_op jit(solution)/shard_map/reshape | solution.py:77
  159.0 21.9 %while.21 = (s32[]{:T(128)}, f32[4,256]{1,0:T(4,128)S(1)}, f32[4,256]{1,0:T(4,128)S(1)}, f32[4,256,128]{2,1,0:T(8,128)S(1)}, f32[4,256]{1,0:T(4,128)S(1)}, /*ind...) while((s32[]{:T(128)}, f32[4,256]{1,0:T(4,128)S(1)}, ...), condition=%wide.region_7.8_spmd.clone, body=%wide.region_0.7_spmd.clone.sunk | while | flops 416944896 | bytes 23601552 | solution.py:94
  159.1 0.6 dynamic_slice.13
  161.0 6.1 %conditional.3 = ((f32[4,256]{1,0:T(4,128)S(1)}, f32[4,256]{1,0:T(4,128)S(1)}, f32[4,256,128]{2,1,0:T(8,128)S(1)}, f32[4,256]{1,0:T(4,128)S(1)}, f32[4,256]{1,0:T(4,128)S(1)}, /*index=5*/f32[4,256,128]{2,1,0:T(8,128)S(1)})) conditional(s32[]{:T(128)} %convert_element_type.38, (f32[4,256]{1,0:T(4,128)S(1)}, f32[4,256]{1,0:T(4,128)S(1)}, ...), branch_computations={%region_1.1_spmd, %region_2.6_spmd} | conditional | flops 416944896 | bytes 23600196 | solution.py:85
  161.0 1.3 dynamic-slice_bitcast_fusion
  162.4 0.5 fusion.27
  162.9 0.1 broadcast_compare_fusion
  163.0 0.7 fusion.3
  163.8 1.0 fusion.7
  164.9 1.1 convolution_add_fusion
  165.9 1.1 convolution_add_fusion.1
  167.1 0.6 dynamic_slice.13
  169.1 0.6 dynamic_slice.13
  171.0 0.6 dynamic_slice.13
  173.0 0.6 dynamic_slice.13
  175.0 0.6 dynamic_slice.13
  177.0 0.6 dynamic_slice.13
  179.0 0.6 dynamic_slice.13
  180.9 0.0 copy-start.5
  180.9 0.0 copy-start.6
  180.9 1.0 copy.18
  181.9 0.2 copy.19
  182.1 0.0 copy-done.5
  182.2 1.2 multiply_reduce_fusion
  183.4 0.0 copy-done.6
  183.4 0.1 multiply_convert_fusion
  183.5 1.7 convolution_convert_fusion
  185.2 0.0 all-reduce.2.cloned.1.call-update
  185.2 60.0 %all-reduce.2.cloned.1.call-done = bf16[256,2048]{1,0:T(8,128)(2,1)} async-done(((bf16[256,2048]{1,0:T(8,128)(2,1)}), bf16[256,2048]{1,0:T(8,128)(2,1)}) %all-reduce.2.cloned.1.call-update) | async-done | bytes 1048592 | tf_op jit(solution)/shard_map/psum | solution.py:108
  245.3 2.3 copy.67
  (40 shorter events, 0.4 us)
Async XLA Ops:
  6.5 177.0 %copy-start = (bf16[512,2048]{1,0:T(8,128)(2,1)S(1)}, bf16[512,2048]{1,0:T(8,128)(2,1)}, u32[]{:S(2)}) copy-start(bf16[512,2048]{1,0:T(8,128)(2,1)} %param.21) | copy-start | bytes 6291460
  6.5 1.7 copy-start.2
  6.5 145.0 %all-gather.2.cloned.1.call-start = ((), (), s32[]{:S(2)}) async-start(), calls=%async_computation | async-start | bytes 8912896 | tf_op jit(solution)/shard_map/all_gather | solution.py:73
  6.5 2.0 copy-start.3
  8.2 1.3 copy-start.4
  8.5 1.7 copy-start.1
  10.2 1.2 copy-start.7
  14.1 231.1 %all-reduce.2.cloned.1.call-start = ((), (), s32[]{:S(2)}) async-start(), calls=%async_computation.1 | async-start | bytes 2097152 | tf_op jit(solution)/shard_map/psum | solution.py:108
  180.9 1.2 copy-start.5
  180.9 2.4 copy-start.6
Sparse Core Ops, SparseCore 0:
  14.3 137.1 all-gather.1
  185.3 59.8 all-reduce.1
where the time goes:
time: 255 us; the launch traced here: 254 us
  waiting for transfers between devices  197 us (77%)
  local copies, waits for them, and re-layouts  23.5 us (9%)
  between operations  13.6 us (5%)
  loops' own time  11.2 us (4%)
  matrix products  6.91 us (3%)
    all_gather x1, waiting for transfers between devices, shards(): kv_piece = lax.all_gather(key_values, 'sp', axis=0, tiled=True)  137 us
    psum x1, waiting for transfers between devices, shards(): result = lax.psum(partial_value.astype(jnp.bfloat16), 'tp')  60 us
    another operation x1, loops' own time, shards(): lax.scan(absorb_step, softmax_state, (stacked, jnp.arange(block_count, dt...  11 us
    reshape x1, local copies, waits for them, and re-layouts, shards(): stacked = kv_piece.reshape(block_count, block_rows, kv_piece.shape[1])  7.41 us
    unnamed x21, local copies, waits for them, and re-layouts  7.03 us
  transfers between devices with their start and end apart: 2, of which 2 were waited for; matrix products, arithmetic and copies ran while one was open for 0% of the time, Pallas kernels for 0%

commit v1 on v0

--- a/solution.py
+++ b/solution.py
@@ -3,6 +3,8 @@
 import jax
 import jax.numpy as jnp
 from jax import lax
+from jax.experimental import pallas as pl
+from jax.experimental.pallas import tpu as pltpu
 from jax.sharding import PartitionSpec as P
 
 epsilon = 1e-06
@@ -109,6 +111,400 @@
     return result
 
 
+MESH = pl.DeviceIdType.MESH
+PLANE = 4
+
+
+def fused_kernel(
+    groups,
+    score_scale,
+    hidden_hbm,
+    q1_hbm,
+    q2_hbm,
+    k1_hbm,
+    k2_hbm,
+    v_hbm,
+    lam_ref,
+    gain_ref,
+    wo_hbm,
+    out_ref,
+    hid,
+    wq1,
+    wq2,
+    wk1,
+    wk2,
+    wv,
+    wo,
+    kv_out,
+    q_out,
+    kv_all,
+    q_all,
+    n_out,
+    n_all,
+    load_sem,
+    wo_send,
+    wo_recv,
+    kv_send,
+    kv_recv,
+    q_send,
+    q_recv,
+    x_send,
+    x_recv,
+    y_send,
+    y_recv,
+    f_send,
+    f_recv,
+    n_send,
+    n_recv,
+):
+    me = lax.axis_index("sp")
+    core = lax.axis_index("tp")
+    plane = me // PLANE
+    spot = lax.rem(me, PLANE)
+    x_spot = spot + 1 - 2 * lax.rem(spot, 2)
+    y_spot = spot + 2 - 4 * (spot // 2)
+    rows = hid.shape[0]
+    qk = q1_hbm.shape[1] // groups
+    width = 2 * qk
+
+    def load(index, src, dst):
+        return pltpu.make_async_copy(src, dst, load_sem.at[index])
+
+    loads = [
+        load(0, hidden_hbm, hid),
+        load(1, k1_hbm, wk1),
+        load(2, k2_hbm, wk2),
+        load(3, v_hbm, wv),
+        load(4, q1_hbm, wq1),
+        load(5, q2_hbm, wq2),
+        load(6, wo_hbm, wo.at[core]),
+    ]
+    for item in loads:
+        item.start()
+
+    barrier = pltpu.get_barrier_semaphore()
+
+    def greet(index, tp_index):
+        pl.semaphore_signal(
+            barrier, inc=1, device_id=(index, tp_index), device_id_type=MESH
+        )
+
+    for step in range(1, groups):
+        other = lax.rem(plane + step, groups) * PLANE + spot
+        greet(other, core)
+        greet(other, 1 - core)
+    greet(me, 1 - core)
+    greet(plane * PLANE + x_spot, core)
+    greet(plane * PLANE + y_spot, core)
+    pl.semaphore_wait(barrier, 2 * (groups - 1) + 3)
+
+    def send(src, dst, send_sem, recv_sem, index, tp_index):
+        return pltpu.make_async_remote_copy(
+            src_ref=src,
+            dst_ref=dst,
+            send_sem=send_sem,
+            recv_sem=recv_sem,
+            device_id=(index, tp_index),
+            device_id_type=MESH,
+        )
+
+    loads[0].wait()
+    pending = []
+
+    def project(weight_ref):
+        return jnp.dot(hid[...], weight_ref[...], preferred_element_type=jnp.float32)
+
+    loads[1].wait()
+    first = project(wk1).astype(jnp.bfloat16)
+    loads[2].wait()
+    second = project(wk2).astype(jnp.bfloat16)
+    for head in range(groups):
+        cut = slice(head * qk, (head + 1) * qk)
+        kv_out[head, :, :width] = jnp.concatenate((first[:, cut], second[:, cut]), axis=1)
+    loads[3].wait()
+    head_v = v_hbm.shape[1] // groups
+    for head in range(groups):
+        cut = slice(head * head_v, (head + 1) * head_v)
+        kv_out[head, :, width:] = jnp.dot(
+            hid[...], wv[:, cut], preferred_element_type=jnp.float32
+        ).astype(jnp.bfloat16)
+    kv_all[me] = kv_out[plane]
+    kv_copies = [None]
+    for step in range(1, groups):
+        target = lax.rem(plane + step, groups)
+        copy = send(
+            kv_out.at[target],
+            kv_all.at[me],
+            kv_send.at[step],
+            kv_recv.at[step],
+            target * PLANE + spot,
+            core,
+        )
+        copy.start()
+        kv_copies.append(copy)
+
+    def from_plane(step):
+        return lax.rem(plane - step + groups, groups)
+
+    def spread(step):
+        block = from_plane(step) * PLANE + spot
+        for sems, where in (((x_send, x_recv), x_spot), ((y_send, y_recv), y_spot)):
+            copy = send(
+                kv_all.at[block],
+                kv_all.at[block],
+                sems[0].at[step],
+                sems[1].at[step],
+                plane * PLANE + where,
+                core,
+            )
+            copy.start()
+            pending.append(copy)
+
+    def arrived(recv_sem, block):
+        pltpu.make_async_copy(kv_all.at[block], kv_all.at[block], recv_sem).wait()
+
+    def relay(step):
+        x_block = from_plane(step) * PLANE + x_spot
+        y_block = from_plane(step) * PLANE + y_spot
+        arrived(x_recv.at[step], x_block)
+        arrived(y_recv.at[step], y_block)
+        block, where = (x_block, y_spot) if step % 2 == 0 else (y_block, x_spot)
+        copy = send(
+            kv_all.at[block],
+            kv_all.at[block],
+            f_send.at[step],
+            f_recv.at[step],
+            plane * PLANE + where,
+            core,
+        )
+        copy.start()
+        pending.append(copy)
+
+    spread(0)
+
+    loads[4].wait()
+    first = (project(wq1) * score_scale).astype(jnp.bfloat16)
+    loads[5].wait()
+    second = (project(wq2) * score_scale).astype(jnp.bfloat16)
+    for head in range(groups):
+        cut = slice(head * qk, (head + 1) * qk)
+        q_out[head] = jnp.concatenate((first[:, cut], second[:, cut]), axis=1)
+    q_all[plane] = q_out[plane]
+    q_copies = [None]
+    for step in range(1, groups):
+        target = lax.rem(plane + step, groups)
+        copy = send(
+            q_out.at[target],
+            q_all.at[plane],
+            q_send.at[step],
+            q_recv.at[step],
+            target * PLANE + spot,
+            core,
+        )
+        copy.start()
+        q_copies.append(copy)
+    loads[6].wait()
+    wo_copy = send(wo.at[core], wo.at[core], wo_send, wo_recv, me, 1 - core)
+    wo_copy.start()
+
+    for step in range(1, groups):
+        arrived(kv_recv.at[step], from_plane(step) * PLANE + spot)
+        spread(step)
+        relay(step - 1)
+    relay(groups - 1)
+    for step in range(groups):
+        arrived(f_recv.at[step], from_plane(step) * PLANE + (PLANE - 1 - spot))
+    for step in range(1, groups):
+        source = from_plane(step)
+        pltpu.make_async_copy(q_all.at[source], q_all.at[source], q_recv.at[step]).wait()
+
+    tile = ROW_TILE
+    chunk = PLANE * rows
+    lane = lax.broadcasted_iota(jnp.int32, (tile, width), 1)
+    lam = lam_ref[plane]
+    gain = gain_ref[...]
+
+    def attend_tile(group, part):
+        begin = pl.multiple_of(part * tile, tile)
+        queries = q_all[group, pl.ds(begin, tile), :]
+        zero = jnp.zeros_like(queries)
+        both = jnp.concatenate(
+            (jnp.where(lane < qk, queries, zero), jnp.where(lane >= qk, queries, zero)), axis=0
+        )
+
+        def absorb(key_group, carry, diagonal):
+            running_max, running_sum, accum = carry
+            block = kv_all[pl.ds(key_group * PLANE, PLANE)].reshape(chunk, width + head_v)
+            scores = lax.dot_general(
+                both,
+                block[:, :width],
+                (((1,), (1,)), ((), ())),
+                preferred_element_type=jnp.float32,
+            )
+            if diagonal:
+                q_pos = spot * rows + begin + lax.rem(
+                    lax.broadcasted_iota(jnp.int32, (2 * tile, chunk), 0), tile
+                )
+                k_pos = lax.broadcasted_iota(jnp.int32, (2 * tile, chunk), 1)
+                scores = jnp.where(k_pos <= q_pos, scores, masked_score)
+            new_max = jnp.maximum(running_max, jnp.max(scores, axis=-1, keepdims=True))
+            weights = jnp.exp2(scores - new_max)
+            rescale = jnp.exp2(running_max - new_max)
+            new_sum = running_sum * rescale + jnp.sum(weights, axis=-1, keepdims=True)
+            added = jnp.dot(
+                weights.astype(jnp.bfloat16),
+                block[:, width:],
+                preferred_element_type=jnp.float32,
+            )
+            return (new_max, new_sum, accum * rescale + added)
+
+        carry = (
+            jnp.full((2 * tile, 1), masked_score, jnp.float32),
+            jnp.zeros((2 * tile, 1), jnp.float32),
+            jnp.zeros((2 * tile, head_v), jnp.float32),
+        )
+        carry = absorb(group, carry, True)
+        carry = lax.fori_loop(0, group, lambda k, c: absorb(k, c, False), carry)
+        heads_out = carry[2] / carry[1]
+        mixed = heads_out[:tile] - lam * heads_out[tile:]
+        scale_rows = lax.rsqrt(jnp.mean(mixed * mixed, axis=-1, keepdims=True) + epsilon)
+        n_out[group, pl.ds(begin, tile), :] = (mixed * scale_rows * gain).astype(jnp.bfloat16)
+
+    def normed_copy(group, tp_index):
+        return send(
+            n_out.at[group],
+            n_all.at[core, plane],
+            n_send.at[group, tp_index],
+            n_recv.at[core, plane],
+            group * PLANE + spot,
+            tp_index,
+        )
+
+    def attend_group(turn, _):
+        group = groups - 1 - turn
+        lax.fori_loop(0, rows // tile, lambda t, c: (attend_tile(group, t), c)[1], 0)
+        normed_copy(group, 1 - core).start()
+
+        @pl.when(group != plane)
+        def _():
+            normed_copy(group, core).start()
+
+        @pl.when(group == plane)
+        def _():
+            n_all[core, plane] = n_out[plane]
+
+        return 0
+
+    lax.fori_loop(0, groups, attend_group, 0)
+
+    wo_copy.wait_send()
+    pltpu.make_async_copy(wo.at[1 - core], wo.at[1 - core], wo_recv).wait()
+    for tp_index in range(2):
+        for head in range(groups):
+
+            @pl.when(jnp.logical_or(head != plane, tp_index != core))
+            def _():
+                slot = n_all.at[tp_index, head]
+                pltpu.make_async_copy(slot, slot, n_recv.at[tp_index, head]).wait()
+
+    halves = [
+        jnp.concatenate([n_all[tp_index, head] for head in range(groups)], axis=1)
+        for tp_index in range(2)
+    ]
+
+    def out_tile(index, _):
+        columns = pl.ds(pl.multiple_of(index * OUT_TILE, OUT_TILE), OUT_TILE)
+        total = None
+        for tp_index in range(2):
+            part = jnp.dot(
+                halves[tp_index], wo[tp_index, :, columns], preferred_element_type=jnp.float32
+            )
+            part = part.astype(jnp.bfloat16).astype(jnp.float32)
+            total = part if total is None else total + part
+        out_ref[:, columns] = total.astype(jnp.bfloat16)
+        return 0
+
+    lax.fori_loop(0, out_ref.shape[1] // OUT_TILE, out_tile, 0)
+
+    for copy in pending:
+        copy.wait_send()
+    for step in range(1, groups):
+        kv_copies[step].wait_send()
+        q_copies[step].wait_send()
+    for group in range(groups):
+        normed_copy(group, 1 - core).wait_send()
+
+        @pl.when(group != plane)
+        def _():
+            normed_copy(group, core).wait_send()
+
+
+ROW_TILE = 128
+OUT_TILE = 256
+
+
+def fused_shards(
+    hidden_in, query_one, query_two, key_one, key_two, value_proj, lambdas, norm_gain, out_proj
+):
+    groups = lambdas.shape[0]
+    rows, depth = hidden_in.shape
+    head_qk = query_one.shape[1] // groups
+    head_v = value_proj.shape[1] // groups
+    width = 2 * head_qk
+    blocks = groups * PLANE
+    columns = out_proj.shape[1]
+    score_scale = 1.75 * head_qk ** (-0.5) * math.log2(math.e)
+    bf16 = jnp.bfloat16
+    dma = pltpu.SemaphoreType.DMA
+    hbm = pl.BlockSpec(memory_space=pl.ANY)
+    vmem = pl.BlockSpec(memory_space=pltpu.VMEM)
+    smem = pl.BlockSpec(memory_space=pltpu.SMEM)
+
+    def body(*refs):
+        fused_kernel(groups, score_scale, *refs)
+
+    return pl.pallas_call(
+        body,
+        name="fused_attention",
+        out_shape=jax.ShapeDtypeStruct((rows, columns), bf16),
+        in_specs=[hbm] * 6 + [smem, vmem, hbm],
+        out_specs=vmem,
+        scratch_shapes=[
+            pltpu.VMEM(hidden_in.shape, bf16),
+            pltpu.VMEM(query_one.shape, bf16),
+            pltpu.VMEM(query_two.shape, bf16),
+            pltpu.VMEM(key_one.shape, bf16),
+            pltpu.VMEM(key_two.shape, bf16),
+            pltpu.VMEM(value_proj.shape, bf16),
+            pltpu.VMEM((2,) + out_proj.shape, bf16),
+            pltpu.VMEM((groups, rows, width + head_v), bf16),
+            pltpu.VMEM((groups, rows, width), bf16),
+            pltpu.VMEM((blocks, rows, width + head_v), bf16),
+            pltpu.VMEM((groups, rows, width), bf16),
+            pltpu.VMEM((groups, rows, head_v), bf16),
+            pltpu.VMEM((2, groups, rows, head_v), bf16),
+            dma((7,)),
+            dma,
+            dma,
+        ]
+        + [dma((groups,))] * 10
+        + [dma((groups, 2)), dma((2, groups))],
+        compiler_params=pltpu.CompilerParams(
+            collective_id=0, has_side_effects=True, vmem_limit_bytes=60 * 1024 * 1024
+        ),
+    )(
+        hidden_in,
+        query_one,
+        query_two,
+        key_one,
+        key_two,
+        value_proj,
+        lambdas,
+        norm_gain.reshape(1, head_v),
+        out_proj,
+    )
+
+
 def solution(mesh):
     placed = (
         P("sp", None),
@@ -121,6 +517,12 @@
         P(),
         P("tp", None),
     )
+
+    def body(*args):
+        groups = args[6].shape[0]
+        split = groups * PLANE == mesh.shape["sp"] and mesh.shape["tp"] == 2
+        return (fused_shards if split else shards)(*args)
+
     return jax.shard_map(
-        shards, mesh=mesh, in_specs=placed, out_specs=P("sp", None), check_vma=False
+        body, mesh=mesh, in_specs=placed, out_specs=P("sp", None), check_vma=False
     )

time: 255 us -> 64 us (0.25)
  waiting for transfers between devices: 197 us -> 0 us
  Pallas kernels: 0 us -> 61.6 us
  local copies, waits for them, and re-layouts: 23.5 us -> 2.3 us
  between operations: 13.6 us -> 0.01 us
  loops' own time: 11.2 us -> 0 us
  matrix products: 6.91 us -> 0 us
    all_gather x1 -> x0, waiting for transfers between devices: 137 us -> none  [shards(): kv_piece = lax.all_gather(key_values, 'sp', axis=0, tiled=True)]
    pallas_call x0 -> x1, Pallas kernels: none -> 61.6 us  [fused_shards(): pl.pallas_call(body, name='fused_attention', out_shape=jax.ShapeDtypeStru...]
    psum x1 -> x0, waiting for transfers between devices: 60 us -> none  [shards(): result = lax.psum(partial_value.astype(jnp.bfloat16), 'tp')]
    another operation x9 -> x0, loops' own time: 11.2 us -> none  [the longest x1 11 us: shards(): lax.scan(absorb_step, softmax_state, (stacked, jnp.arange(block_count, dt...]
    reshape x1 -> x0, local copies, waits for them, and re-layouts: 7.41 us -> none  [shards(): stacked = kv_piece.reshape(block_count, block_rows, kv_piece.shape[1])]
    dot_general x6 -> x0, matrix products: 6.91 us -> none  [the longest x2 2.14 us: one_map(): jnp.einsum('hqk,khe->hqe', weights.astype(jnp.bfloat16), value_rows, pref...]
    unnamed x21 -> x1, local copies, waits for them, and re-layouts: 7.03 us -> 2.3 us
    dynamic_slice x8 -> x0, local copies, waits for them, and re-layouts: 4.69 us -> none  [shards(): lax.scan(absorb_step, softmax_state, (stacked, jnp.arange(block_count, dt...]
  transfers between devices with their start and end apart: 2 -> 0, of which waited for: 2 -> 0; matrix products, arithmetic and copies ran while one was open for 0% -> 0% of each run, Pallas kernels for 0% -> 0%
where the time goes in v1:
time: 64 us; the launch traced here: 63.9 us
  Pallas kernels  61.6 us (96%)
  local copies, waits for them, and re-layouts  2.3 us (4%)
    pallas_call x1, Pallas kernels, fused_shards(): pl.pallas_call(body, name='fused_attention', out_shape=jax.ShapeDtypeStru...  61.6 us
    unnamed x1, local copies, waits for them, and re-layouts  2.3 us

profile of v1, /device:TPU:0, one launch (start us, length us, event | category | flops | bytes accessed | tf_op | source)
XLA Modules:
  0.0 63.9 jit_solution(14810163804121498571)
XLA Ops:
  0.0 61.6 %fused_attention.1 = bf16[256,2048]{1,0:T(8,128)(2,1)} custom-call(bf16[256,2048]{1,0:T(8,128)(2,1)} %refs_0_.1, bf16[2048,256]{1,0:T(8,128)(2,1)} %refs_1_.1, bf16[2048,256]{1,0:T(8,128)(2,1)} %refs_2_.1, bf16[2048,256]{1,0:T(8,128)(2,1)} %refs_3_.1, bf16[2048,256]{1,0:T(8,128)(2,1)} %refs_4_.1, bf16[2048,512]{1,0:T(8,128)(2,1)} %refs_5_.1, f32[4]{0:T(128)} %refs_6_.1, ...), custom_call_target="tpu_custom_call" | custom-call | tf_op jit(solution)/shard_map/fused_attention/pallas_call | solution.py:466
  61.6 2.3 %copy.11 = bf16[256,2048]{1,0:T(8,128)(2,1)} copy(bf16[256,2048]{1,0:T(8,128)(2,1)} %fused_attention.1) | data formatting | bytes 2097152

commit v2 on v1

--- a/solution.py
+++ b/solution.py
@@ -141,6 +141,9 @@
     q_all,
     n_out,
     n_all,
+    max_all,
+    sum_all,
+    acc_all,
     load_sem,
     wo_send,
     wo_recv,
@@ -156,6 +159,8 @@
     f_recv,
     n_send,
     n_recv,
+    r_send,
+    r_recv,
 ):
     me = lax.axis_index("sp")
     core = lax.axis_index("tp")
@@ -179,9 +184,6 @@
         load(5, q2_hbm, wq2),
         load(6, wo_hbm, wo.at[core]),
     ]
-    for item in loads:
-        item.start()
-
     barrier = pltpu.get_barrier_semaphore()
 
     def greet(index, tp_index):
@@ -192,11 +194,12 @@
     for step in range(1, groups):
         other = lax.rem(plane + step, groups) * PLANE + spot
         greet(other, core)
-        greet(other, 1 - core)
     greet(me, 1 - core)
     greet(plane * PLANE + x_spot, core)
     greet(plane * PLANE + y_spot, core)
-    pl.semaphore_wait(barrier, 2 * (groups - 1) + 3)
+
+    for item in loads:
+        item.start()
 
     def send(src, dst, send_sem, recv_sem, index, tp_index):
         return pltpu.make_async_remote_copy(
@@ -229,6 +232,7 @@
             hid[...], wv[:, cut], preferred_element_type=jnp.float32
         ).astype(jnp.bfloat16)
     kv_all[me] = kv_out[plane]
+    pl.semaphore_wait(barrier, groups - 1 + 3)
     kv_copies = [None]
     for step in range(1, groups):
         target = lax.rem(plane + step, groups)
@@ -307,136 +311,160 @@
     wo_copy = send(wo.at[core], wo.at[core], wo_send, wo_recv, me, 1 - core)
     wo_copy.start()
 
-    for step in range(1, groups):
+    def forward_arrival(step):
         arrived(kv_recv.at[step], from_plane(step) * PLANE + spot)
         spread(step)
-        relay(step - 1)
-    relay(groups - 1)
-    for step in range(groups):
+
+    def stage_ready(step):
         arrived(f_recv.at[step], from_plane(step) * PLANE + (PLANE - 1 - spot))
-    for step in range(1, groups):
-        source = from_plane(step)
-        pltpu.make_async_copy(q_all.at[source], q_all.at[source], q_recv.at[step]).wait()
+        if step > 0:
+            slot = q_all.at[from_plane(step)]
+            pltpu.make_async_copy(slot, slot, q_recv.at[step]).wait()
 
     tile = ROW_TILE
+    tiles = rows // tile
     chunk = PLANE * rows
     lane = lax.broadcasted_iota(jnp.int32, (tile, width), 1)
     lam = lam_ref[plane]
     gain = gain_ref[...]
 
-    def attend_tile(group, part):
+    def pair_tile(group, key_group, part, diagonal):
         begin = pl.multiple_of(part * tile, tile)
         queries = q_all[group, pl.ds(begin, tile), :]
         zero = jnp.zeros_like(queries)
         both = jnp.concatenate(
             (jnp.where(lane < qk, queries, zero), jnp.where(lane >= qk, queries, zero)), axis=0
         )
-
-        def absorb(key_group, carry, diagonal):
-            running_max, running_sum, accum = carry
-            block = kv_all[pl.ds(key_group * PLANE, PLANE)].reshape(chunk, width + head_v)
-            scores = lax.dot_general(
-                both,
-                block[:, :width],
-                (((1,), (1,)), ((), ())),
-                preferred_element_type=jnp.float32,
+        block = kv_all[pl.ds(key_group * PLANE, PLANE)].reshape(chunk, width + head_v)
+        scores = lax.dot_general(
+            both,
+            block[:, :width],
+            (((1,), (1,)), ((), ())),
+            preferred_element_type=jnp.float32,
+        )
+        if diagonal:
+            q_pos = spot * rows + begin + lax.rem(
+                lax.broadcasted_iota(jnp.int32, (2 * tile, chunk), 0), tile
             )
-            if diagonal:
-                q_pos = spot * rows + begin + lax.rem(
-                    lax.broadcasted_iota(jnp.int32, (2 * tile, chunk), 0), tile
-                )
-                k_pos = lax.broadcasted_iota(jnp.int32, (2 * tile, chunk), 1)
-                scores = jnp.where(k_pos <= q_pos, scores, masked_score)
-            new_max = jnp.maximum(running_max, jnp.max(scores, axis=-1, keepdims=True))
-            weights = jnp.exp2(scores - new_max)
+            k_pos = lax.broadcasted_iota(jnp.int32, (2 * tile, chunk), 1)
+            scores = jnp.where(k_pos <= q_pos, scores, masked_score)
+        new_max = jnp.max(scores, axis=-1, keepdims=True)
+        if not diagonal:
+            running_max = max_all[group, part]
+            new_max = jnp.maximum(running_max, new_max)
             rescale = jnp.exp2(running_max - new_max)
-            new_sum = running_sum * rescale + jnp.sum(weights, axis=-1, keepdims=True)
-            added = jnp.dot(
-                weights.astype(jnp.bfloat16),
-                block[:, width:],
-                preferred_element_type=jnp.float32,
-            )
-            return (new_max, new_sum, accum * rescale + added)
-
-        carry = (
-            jnp.full((2 * tile, 1), masked_score, jnp.float32),
-            jnp.zeros((2 * tile, 1), jnp.float32),
-            jnp.zeros((2 * tile, head_v), jnp.float32),
-        )
-        carry = absorb(group, carry, True)
-        carry = lax.fori_loop(0, group, lambda k, c: absorb(k, c, False), carry)
-        heads_out = carry[2] / carry[1]
-        mixed = heads_out[:tile] - lam * heads_out[tile:]
-        scale_rows = lax.rsqrt(jnp.mean(mixed * mixed, axis=-1, keepdims=True) + epsilon)
-        n_out[group, pl.ds(begin, tile), :] = (mixed * scale_rows * gain).astype(jnp.bfloat16)
-
-    def normed_copy(group, tp_index):
+        weights = jnp.exp2(scores - new_max)
+        new_sum = jnp.sum(weights, axis=-1, keepdims=True)
+        accum = jnp.dot(
+            weights.astype(jnp.bfloat16),
+            block[:, width:],
+            preferred_element_type=jnp.float32,
+        )
+        if not diagonal:
+            new_sum = sum_all[group, part] * rescale + new_sum
+            accum = acc_all[group, part] * rescale + accum
+        max_all[group, part] = new_max
+        sum_all[group, part] = new_sum
+        acc_all[group, part] = accum
+
+    def pair(group, key_group, diagonal):
+        lax.fori_loop(
+            0, tiles, lambda t, c: (pair_tile(group, key_group, t, diagonal), c)[1], 0
+        )
+
+    def meet(step, earlier):
+        one, other = from_plane(step), from_plane(earlier)
+        pair(jnp.maximum(one, other), jnp.minimum(one, other), False)
+
+    def normed_copy(group):
         return send(
             n_out.at[group],
             n_all.at[core, plane],
-            n_send.at[group, tp_index],
-            n_recv.at[core, plane],
+            n_send.at[group],
+            n_recv.at[plane],
             group * PLANE + spot,
-            tp_index,
-        )
-
-    def attend_group(turn, _):
-        group = groups - 1 - turn
-        lax.fori_loop(0, rows // tile, lambda t, c: (attend_tile(group, t), c)[1], 0)
-        normed_copy(group, 1 - core).start()
-
-        @pl.when(group != plane)
-        def _():
-            normed_copy(group, core).start()
-
-        @pl.when(group == plane)
-        def _():
-            n_all[core, plane] = n_out[plane]
-
-        return 0
-
-    lax.fori_loop(0, groups, attend_group, 0)
-
+            core,
+        )
+
+    def partner_copy(head):
+        slot = n_all.at[core, head]
+        return send(slot, slot, r_send.at[head], r_recv.at[head], me, 1 - core)
+
+    def finish(group):
+        def finish_tile(part, _):
+            begin = pl.multiple_of(part * tile, tile)
+            heads_out = acc_all[group, part] / sum_all[group, part]
+            mixed = heads_out[:tile] - lam * heads_out[tile:]
+            scale_rows = lax.rsqrt(jnp.mean(mixed * mixed, axis=-1, keepdims=True) + epsilon)
+            normed = (mixed * scale_rows * gain).astype(jnp.bfloat16)
+            n_out[group, pl.ds(begin, tile), :] = normed
+            return 0
+
+        lax.fori_loop(0, tiles, finish_tile, 0)
+
+    forward_arrival(1)
+    relay(0)
+    stage_ready(0)
+    pair(plane, plane, True)
+    for step in range(1, groups):
+        if step + 1 < groups:
+            forward_arrival(step + 1)
+        relay(step)
+        stage_ready(step)
+        pair(from_plane(step), from_plane(step), True)
+        if step + 1 < groups:
+            for earlier in range(step):
+                meet(step, earlier)
+        else:
+            for earlier in list(range(1, step)) + [0]:
+                meet(step, earlier)
+                finish(from_plane(earlier))
+                if earlier == 0:
+                    n_all[core, plane] = n_out[plane]
+                    partner_copy(plane).start()
+                else:
+                    normed_copy(from_plane(earlier)).start()
+    finish(from_plane(groups - 1))
+    normed_copy(from_plane(groups - 1)).start()
+
+    for step in range(1, groups):
+        head = from_plane(step)
+        slot = n_all.at[core, head]
+        pltpu.make_async_copy(slot, slot, n_recv.at[head]).wait()
+        partner_copy(head).start()
     wo_copy.wait_send()
+
+    def out_tiles(tp_index, first_part):
+        normed = jnp.concatenate([n_all[tp_index, head] for head in range(groups)], axis=1)
+
+        def out_tile(index, _):
+            columns = pl.ds(pl.multiple_of(index * OUT_TILE, OUT_TILE), OUT_TILE)
+            part = jnp.dot(normed, wo[tp_index, :, columns], preferred_element_type=jnp.float32)
+            part = part.astype(jnp.bfloat16)
+            if not first_part:
+                part = (part.astype(jnp.float32) + out_ref[:, columns].astype(jnp.float32)).astype(
+                    jnp.bfloat16
+                )
+            out_ref[:, columns] = part
+            return 0
+
+        lax.fori_loop(0, out_ref.shape[1] // OUT_TILE, out_tile, 0)
+
+    out_tiles(core, True)
     pltpu.make_async_copy(wo.at[1 - core], wo.at[1 - core], wo_recv).wait()
-    for tp_index in range(2):
-        for head in range(groups):
-
-            @pl.when(jnp.logical_or(head != plane, tp_index != core))
-            def _():
-                slot = n_all.at[tp_index, head]
-                pltpu.make_async_copy(slot, slot, n_recv.at[tp_index, head]).wait()
-
-    halves = [
-        jnp.concatenate([n_all[tp_index, head] for head in range(groups)], axis=1)
-        for tp_index in range(2)
-    ]
-
-    def out_tile(index, _):
-        columns = pl.ds(pl.multiple_of(index * OUT_TILE, OUT_TILE), OUT_TILE)
-        total = None
-        for tp_index in range(2):
-            part = jnp.dot(
-                halves[tp_index], wo[tp_index, :, columns], preferred_element_type=jnp.float32
-            )
-            part = part.astype(jnp.bfloat16).astype(jnp.float32)
-            total = part if total is None else total + part
-        out_ref[:, columns] = total.astype(jnp.bfloat16)
-        return 0
-
-    lax.fori_loop(0, out_ref.shape[1] // OUT_TILE, out_tile, 0)
+    for head in range(groups):
+        slot = n_all.at[1 - core, head]
+        pltpu.make_async_copy(slot, slot, r_recv.at[head]).wait()
+    out_tiles(1 - core, False)
 
     for copy in pending:
         copy.wait_send()
     for step in range(1, groups):
         kv_copies[step].wait_send()
         q_copies[step].wait_send()
-    for group in range(groups):
-        normed_copy(group, 1 - core).wait_send()
-
-        @pl.when(group != plane)
-        def _():
-            normed_copy(group, core).wait_send()
+        normed_copy(from_plane(step)).wait_send()
+    for head in range(groups):
+        partner_copy(head).wait_send()
 
 
 ROW_TILE = 128
@@ -483,12 +511,14 @@
             pltpu.VMEM((groups, rows, width), bf16),
             pltpu.VMEM((groups, rows, head_v), bf16),
             pltpu.VMEM((2, groups, rows, head_v), bf16),
+            pltpu.VMEM((groups, rows // ROW_TILE, 2 * ROW_TILE, 1), jnp.float32),
+            pltpu.VMEM((groups, rows // ROW_TILE, 2 * ROW_TILE, 1), jnp.float32),
+            pltpu.VMEM((groups, rows // ROW_TILE, 2 * ROW_TILE, head_v), jnp.float32),
             dma((7,)),
             dma,
             dma,
         ]
-        + [dma((groups,))] * 10
-        + [dma((groups, 2)), dma((2, groups))],
+        + [dma((groups,))] * 14,
         compiler_params=pltpu.CompilerParams(
             collective_id=0, has_side_effects=True, vmem_limit_bytes=60 * 1024 * 1024
         ),

time: 64 us -> 67.8 us (1.059)
  Pallas kernels: 61.6 us -> 65.3 us
    pallas_call x1, Pallas kernels: 61.6 us -> 65.3 us  [fused_shards(): pl.pallas_call(body, name='fused_attention', out_shape=jax.ShapeDtypeStru...]
where the time goes in v2:
time: 67.8 us; the launch traced here: 67.6 us
  Pallas kernels  65.3 us (96%)
  local copies, waits for them, and re-layouts  2.3 us (3%)
    pallas_call x1, Pallas kernels, fused_shards(): pl.pallas_call(body, name='fused_attention', out_shape=jax.ShapeDtypeStru...  65.3 us
    unnamed x1, local copies, waits for them, and re-layouts  2.3 us

profile of v2, /device:TPU:0, one launch (start us, length us, event | category | flops | bytes accessed | tf_op | source)
XLA Modules:
  0.0 67.6 jit_solution(8587349818225678958)
XLA Ops:
  0.0 65.3 %fused_attention.1 = bf16[256,2048]{1,0:T(8,128)(2,1)} custom-call(bf16[256,2048]{1,0:T(8,128)(2,1)} %refs_0_.1, bf16[2048,256]{1,0:T(8,128)(2,1)} %refs_1_.1, bf16[2048,256]{1,0:T(8,128)(2,1)} %refs_2_.1, bf16[2048,256]{1,0:T(8,128)(2,1)} %refs_3_.1, bf16[2048,256]{1,0:T(8,128)(2,1)} %refs_4_.1, bf16[2048,512]{1,0:T(8,128)(2,1)} %refs_5_.1, f32[4]{0:T(128)} %refs_6_.1, ...), custom_call_target="tpu_custom_call" | custom-call | tf_op jit(solution)/shard_map/fused_attention/pallas_call | solution.py:494
  65.3 2.3 %copy.11 = bf16[256,2048]{1,0:T(8,128)(2,1)} copy(bf16[256,2048]{1,0:T(8,128)(2,1)} %fused_attention.1) | data formatting | bytes 2097152

commit v3 on v2

--- a/solution.py
+++ b/solution.py
@@ -211,6 +211,15 @@
             device_id_type=MESH,
         )
 
+    upper = plane >= groups // 2
+    mirrored = jnp.where(upper, groups - 1 - plane, plane)
+
+    def from_plane(step):
+        if step == 0:
+            return plane
+        near = jnp.where(step - 1 < mirrored, step - 1, step)
+        return jnp.where(upper, groups - 1 - near, near)
+
     loads[0].wait()
     pending = []
 
@@ -232,23 +241,37 @@
             hid[...], wv[:, cut], preferred_element_type=jnp.float32
         ).astype(jnp.bfloat16)
     kv_all[me] = kv_out[plane]
+    loads[4].wait()
+    first = (project(wq1) * score_scale).astype(jnp.bfloat16)
+    loads[5].wait()
+    second = (project(wq2) * score_scale).astype(jnp.bfloat16)
+    for head in range(groups):
+        cut = slice(head * qk, (head + 1) * qk)
+        q_out[head] = jnp.concatenate((first[:, cut], second[:, cut]), axis=1)
+    q_all[plane] = q_out[plane]
     pl.semaphore_wait(barrier, groups - 1 + 3)
-    kv_copies = [None]
-    for step in range(1, groups):
-        target = lax.rem(plane + step, groups)
-        copy = send(
+
+    def kv_copy(step):
+        target = from_plane(step)
+        return send(
             kv_out.at[target],
             kv_all.at[me],
             kv_send.at[step],
-            kv_recv.at[step],
+            kv_recv.at[plane],
             target * PLANE + spot,
             core,
         )
-        copy.start()
-        kv_copies.append(copy)
-
-    def from_plane(step):
-        return lax.rem(plane - step + groups, groups)
+
+    def q_copy(step):
+        target = from_plane(step)
+        return send(
+            q_out.at[target],
+            q_all.at[plane],
+            q_send.at[step],
+            q_recv.at[plane],
+            target * PLANE + spot,
+            core,
+        )
 
     def spread(step):
         block = from_plane(step) * PLANE + spot
@@ -267,59 +290,50 @@
     def arrived(recv_sem, block):
         pltpu.make_async_copy(kv_all.at[block], kv_all.at[block], recv_sem).wait()
 
+    half = rows // 2
+
     def relay(step):
         x_block = from_plane(step) * PLANE + x_spot
         y_block = from_plane(step) * PLANE + y_spot
-        arrived(x_recv.at[step], x_block)
-        arrived(y_recv.at[step], y_block)
-        block, where = (x_block, y_spot) if step % 2 == 0 else (y_block, x_spot)
-        copy = send(
-            kv_all.at[block],
-            kv_all.at[block],
-            f_send.at[step],
-            f_recv.at[step],
-            plane * PLANE + where,
-            core,
-        )
-        copy.start()
-        pending.append(copy)
-
+        for part, block, sem, where in (
+            (0, x_block, x_recv, y_spot),
+            (1, y_block, y_recv, x_spot),
+        ):
+            arrived(sem.at[step], block)
+            piece = kv_all.at[block, pl.ds(part * half, half), :]
+            copy = send(
+                piece,
+                piece,
+                f_send.at[step, part],
+                f_recv.at[step, part],
+                plane * PLANE + where,
+                core,
+            )
+            copy.start()
+            pending.append(copy)
+
+    kv_copy(1).start()
     spread(0)
-
-    loads[4].wait()
-    first = (project(wq1) * score_scale).astype(jnp.bfloat16)
-    loads[5].wait()
-    second = (project(wq2) * score_scale).astype(jnp.bfloat16)
-    for head in range(groups):
-        cut = slice(head * qk, (head + 1) * qk)
-        q_out[head] = jnp.concatenate((first[:, cut], second[:, cut]), axis=1)
-    q_all[plane] = q_out[plane]
-    q_copies = [None]
-    for step in range(1, groups):
-        target = lax.rem(plane + step, groups)
-        copy = send(
-            q_out.at[target],
-            q_all.at[plane],
-            q_send.at[step],
-            q_recv.at[step],
-            target * PLANE + spot,
-            core,
-        )
-        copy.start()
-        q_copies.append(copy)
+    for step in range(2, groups):
+        kv_copy(step).start()
+        q_copy(step - 1).start()
+    q_copy(groups - 1).start()
     loads[6].wait()
     wo_copy = send(wo.at[core], wo.at[core], wo_send, wo_recv, me, 1 - core)
     wo_copy.start()
 
     def forward_arrival(step):
-        arrived(kv_recv.at[step], from_plane(step) * PLANE + spot)
+        arrived(kv_recv.at[from_plane(step)], from_plane(step) * PLANE + spot)
         spread(step)
 
     def stage_ready(step):
-        arrived(f_recv.at[step], from_plane(step) * PLANE + (PLANE - 1 - spot))
+        far = from_plane(step) * PLANE + (PLANE - 1 - spot)
+        for part in range(2):
+            piece = kv_all.at[far, pl.ds(part * half, half), :]
+            pltpu.make_async_copy(piece, piece, f_recv.at[step, part]).wait()
         if step > 0:
             slot = q_all.at[from_plane(step)]
-            pltpu.make_async_copy(slot, slot, q_recv.at[step]).wait()
+            pltpu.make_async_copy(slot, slot, q_recv.at[from_plane(step)]).wait()
 
     tile = ROW_TILE
     tiles = rows // tile
@@ -402,14 +416,7 @@
 
         lax.fori_loop(0, tiles, finish_tile, 0)
 
-    forward_arrival(1)
-    relay(0)
-    stage_ready(0)
-    pair(plane, plane, True)
-    for step in range(1, groups):
-        if step + 1 < groups:
-            forward_arrival(step + 1)
-        relay(step)
+    def stage(step):
         stage_ready(step)
         pair(from_plane(step), from_plane(step), True)
         if step + 1 < groups:
@@ -424,6 +431,15 @@
                     partner_copy(plane).start()
                 else:
                     normed_copy(from_plane(earlier)).start()
+
+    for step in range(1, groups):
+        forward_arrival(step)
+        relay(step - 1)
+        if step >= 2:
+            stage(step - 2)
+    relay(groups - 1)
+    stage(groups - 2)
+    stage(groups - 1)
     finish(from_plane(groups - 1))
     normed_copy(from_plane(groups - 1)).start()
 
@@ -460,14 +476,14 @@
     for copy in pending:
         copy.wait_send()
     for step in range(1, groups):
-        kv_copies[step].wait_send()
-        q_copies[step].wait_send()
+        kv_copy(step).wait_send()
+        q_copy(step).wait_send()
         normed_copy(from_plane(step)).wait_send()
     for head in range(groups):
         partner_copy(head).wait_send()
 
 
-ROW_TILE = 128
+ROW_TILE = 256
 OUT_TILE = 256
 
 
@@ -518,7 +534,9 @@
             dma,
             dma,
         ]
-        + [dma((groups,))] * 14,
+        + [dma((groups,))] * 8
+        + [dma((groups, 2))] * 2
+        + [dma((groups,))] * 4,
         compiler_params=pltpu.CompilerParams(
             collective_id=0, has_side_effects=True, vmem_limit_bytes=60 * 1024 * 1024
         ),

time: 67.8 us -> 57.7 us (0.85)
  Pallas kernels: 65.3 us -> 55.3 us
    pallas_call x1, Pallas kernels: 65.3 us -> 55.3 us  [fused_shards(): pl.pallas_call(body, name='fused_attention', out_shape=jax.ShapeDtypeStru...]
where the time goes in v3:
time: 57.7 us; the launch traced here: 57.6 us
  Pallas kernels  55.3 us (96%)
  local copies, waits for them, and re-layouts  2.3 us (4%)
    pallas_call x1, Pallas kernels, fused_shards(): pl.pallas_call(body, name='fused_attention', out_shape=jax.ShapeDtypeStru...  55.3 us
    unnamed x1, local copies, waits for them, and re-layouts  2.3 us

profile of v3, /device:TPU:0, one launch (start us, length us, event | category | flops | bytes accessed | tf_op | source)
XLA Modules:
  0.0 57.6 jit_solution(2872703873733514704)
XLA Ops:
  0.0 55.3 %fused_attention.1 = bf16[256,2048]{1,0:T(8,128)(2,1)} custom-call(bf16[256,2048]{1,0:T(8,128)(2,1)} %refs_0_.1, bf16[2048,256]{1,0:T(8,128)(2,1)} %refs_1_.1, bf16[2048,256]{1,0:T(8,128)(2,1)} %refs_2_.1, bf16[2048,256]{1,0:T(8,128)(2,1)} %refs_3_.1, bf16[2048,256]{1,0:T(8,128)(2,1)} %refs_4_.1, bf16[2048,512]{1,0:T(8,128)(2,1)} %refs_5_.1, f32[4]{0:T(128)} %refs_6_.1, ...), custom_call_target="tpu_custom_call" | custom-call | tf_op jit(solution)/shard_map/fused_attention/pallas_call | solution.py:510
  55.3 2.3 %copy.11 = bf16[256,2048]{1,0:T(8,128)(2,1)} copy(bf16[256,2048]{1,0:T(8,128)(2,1)} %fused_attention.1) | data formatting | bytes 2097152

commit v4 on v3

--- a/solution.py
+++ b/solution.py
@@ -484,7 +484,7 @@
 
 
 ROW_TILE = 256
-OUT_TILE = 256
+OUT_TILE = 1024
 
 
 def fused_shards(

time: 57.7 us -> 55.7 us (0.965)
  Pallas kernels: 55.3 us -> 53.2 us
    pallas_call x1, Pallas kernels: 55.3 us -> 53.2 us  [fused_shards(): pl.pallas_call(body, name='fused_attention', out_shape=jax.ShapeDtypeStru...]
where the time goes in v4:
time: 55.7 us; the launch traced here: 55.5 us
  Pallas kernels  53.2 us (96%)
  local copies, waits for them, and re-layouts  2.3 us (4%)
    pallas_call x1, Pallas kernels, fused_shards(): pl.pallas_call(body, name='fused_attention', out_shape=jax.ShapeDtypeStru...  53.2 us
    unnamed x1, local copies, waits for them, and re-layouts  2.3 us

profile of v4, /device:TPU:0, one launch (start us, length us, event | category | flops | bytes accessed | tf_op | source)
XLA Modules:
  0.0 55.5 jit_solution(9074404866692884829)
XLA Ops:
  0.0 53.2 %fused_attention.1 = bf16[256,2048]{1,0:T(8,128)(2,1)} custom-call(bf16[256,2048]{1,0:T(8,128)(2,1)} %refs_0_.1, bf16[2048,256]{1,0:T(8,128)(2,1)} %refs_1_.1, bf16[2048,256]{1,0:T(8,128)(2,1)} %refs_2_.1, bf16[2048,256]{1,0:T(8,128)(2,1)} %refs_3_.1, bf16[2048,256]{1,0:T(8,128)(2,1)} %refs_4_.1, bf16[2048,512]{1,0:T(8,128)(2,1)} %refs_5_.1, f32[4]{0:T(128)} %refs_6_.1, ...), custom_call_target="tpu_custom_call" | custom-call | tf_op jit(solution)/shard_map/fused_attention/pallas_call | solution.py:510
  53.2 2.3 %copy.11 = bf16[256,2048]{1,0:T(8,128)(2,1)} copy(bf16[256,2048]{1,0:T(8,128)(2,1)} %fused_attention.1) | data formatting | bytes 2097152
